TPU v7x, 32 devices: a whole 2x2x4 slice. The times are simulated.
32 devices in a mesh: sp: 8 (over z, y), tp: 4 (over x, core).
Axes of the slice: x: 2, y: 2, z: 4, core: 2. Of those that a mesh axis runs over, the one named last changes fastest.
Arguments:
- queries: bfloat16 [4096, 2048], P('sp', 'tp'), may hold values from -6 to 6
- keys: bfloat16 [4096, 512], P('sp', 'tp'), may hold values from -6 to 6
- values: bfloat16 [4096, 512], P('sp', 'tp'), may hold values from -6 to 6
- residual: bfloat16 [4096, 2048], P(('sp', 'tp')), may hold values from -0.119628906 to 0.119628906
- out_proj: bfloat16 [2048, 2048], replicated, may hold values from -0.125 to 0.125
- query_gain: float32 [128], replicated, may hold values from 0.7 to 7
- key_gain: float32 [128], replicated, may hold values from 0.7 to 7
- norm_gain: float32 [2048], replicated, may hold values from 0.1 to 1.9
- routes: int32 [4096, 4], P(('sp', 'tp')), may hold values from 0 to 31, all different within a row; in each aligned block of 128 rows (0 to 127, 128 to 255, ...) at most 32 rows name the same one
- route_weight: float32 [4096, 4], P(('sp', 'tp')), may hold values from 0.1 to 1
- expert_gate: bfloat16 [32, 2048, 256], P(('sp', 'tp')), may hold values from -0.125 to 0.125
- expert_up: bfloat16 [32, 2048, 256], P(('sp', 'tp')), may hold values from -0.125 to 0.125
- expert_down: bfloat16 [32, 256, 2048], P(('sp', 'tp')), may hold values from -0.375 to 0.375
- shared_gate: bfloat16 [2048, 256], replicated, may hold values from -0.125 to 0.125
- shared_up: bfloat16 [2048, 256], replicated, may hold values from -0.125 to 0.125
- shared_down: bfloat16 [256, 2048], replicated, may hold values from -0.375 to 0.375
Outputs:
- layer_out: bfloat16 [4096, 2048], P(('sp', 'tp'))
Inputs may be any that keep to these rules, and one draw needn't show every extreme that they name: In the rows of one device (aligned blocks of 128 tokens), no expert is named by more than 32 routes; some expert is named by exactly 32 routes of some device; the 4 experts of a token differ.
All inputs are finite; a program needn't handle non-finite values.
Results may differ from a plain program's by a relative error of at most 0.023.
The roundings to bfloat16 on the way count: a program that leaves them out, or rounds other values in their place, can miss the bound.
Values may be sent and summed in bfloat16 or wider, within the bound.
A program may use at most 128 MiB of HBM per device.

v0:
```python
import math
import jax
import jax.numpy as jnp
from jax import lax
from jax.sharding import PartitionSpec as P

HEADS = 16
KV_HEADS = 4
GRID_W = 64
EPS = 1e-06
THETA = 10000.0


def rotate_pairs(block, cosine, sine):
    first, second = jnp.split(block, 2, axis=-1)
    return jnp.concatenate(
        [first * cosine - second * sine, second * cosine + first * sine], axis=-1
    )


def normed_rotary(source, gain, heads, offset):
    count = source.shape[0]
    width = gain.shape[0]
    values_f = source.astype(jnp.float32).reshape(count, heads, width)
    values_f = (
        values_f * lax.rsqrt(jnp.mean(values_f * values_f, axis=-1, keepdims=True) + EPS) * gain
    )
    position = offset + jnp.arange(count, dtype=jnp.int32)
    grid_row = (position // GRID_W).astype(jnp.float32)
    grid_col = (position % GRID_W).astype(jnp.float32)
    quarter = width // 4
    inverse = jnp.power(THETA, -4.0 * jnp.arange(quarter, dtype=jnp.float32) / width)
    row_angle = (grid_row[:, None] * inverse[None, :])[:, None, :]
    col_angle = (grid_col[:, None] * inverse[None, :])[:, None, :]
    row_half, col_half = jnp.split(values_f, 2, axis=-1)
    turned = jnp.concatenate(
        [
            rotate_pairs(row_half, jnp.cos(row_angle), jnp.sin(row_angle)),
            rotate_pairs(col_half, jnp.cos(col_angle), jnp.sin(col_angle)),
        ],
        axis=-1,
    )
    return turned.reshape(count, heads * width).astype(jnp.bfloat16)


def expert_apply(arrived, expert_gate, expert_up, expert_down):
    sources, slots, width = arrived.shape
    local = expert_gate.shape[0]
    grouped = arrived.reshape(sources // local, local, slots, width)
    gate_part = jnp.einsum(
        "sech,ehf->secf", grouped, expert_gate, preferred_element_type=jnp.float32
    )
    up_part = jnp.einsum("sech,ehf->secf", grouped, expert_up, preferred_element_type=jnp.float32)
    hidden_e = (jax.nn.silu(gate_part) * up_part).astype(jnp.bfloat16)
    result = jnp.einsum("secf,efh->sech", hidden_e, expert_down, preferred_element_type=jnp.float32)
    return result.astype(jnp.bfloat16).reshape(sources, slots, width)


def body(
    queries,
    keys,
    values,
    residual,
    out_proj,
    query_gain,
    key_gain,
    norm_gain,
    routes,
    route_weight,
    expert_gate,
    expert_up,
    expert_down,
    shared_gate,
    shared_up,
    shared_down,
):
    tok_local = queries.shape[0]
    width = query_gain.shape[0]
    group = HEADS // KV_HEADS
    kv_local = keys.shape[1] // width
    scale = 1.0 / math.sqrt(width)
    offset = lax.axis_index("sp") * tok_local
    q_rot = normed_rotary(queries, query_gain, kv_local * group, offset)
    k_rot = normed_rotary(keys, key_gain, kv_local, offset)
    query_3d = q_rot.reshape(tok_local, kv_local, group, width).transpose(1, 2, 0, 3)
    query_3d = query_3d.reshape(kv_local, group * tok_local, width)
    start_state = (
        jnp.full((kv_local, group * tok_local), -jnp.inf, jnp.float32),
        jnp.zeros((kv_local, group * tok_local), jnp.float32),
        jnp.zeros((kv_local, group * tok_local, width), jnp.float32),
    )
    key_piece = lax.all_gather(k_rot, "sp", axis=0, tiled=True)
    value_piece = lax.all_gather(values, "sp", axis=0, tiled=True)
    count = key_piece.shape[0]
    block = math.gcd(count, 512)

    def one_block(index_block, state):
        running_max, running_sum, accum = state
        key_rows = lax.dynamic_slice_in_dim(key_piece, index_block * block, block, 0)
        value_rows = lax.dynamic_slice_in_dim(value_piece, index_block * block, block, 0)
        key_3d = key_rows.reshape(block, kv_local, width)
        value_3d = value_rows.reshape(block, kv_local, width)
        scores = (
            jnp.einsum("gqd,kgd->gqk", query_3d, key_3d, preferred_element_type=jnp.float32) * scale
        )
        new_max = jnp.maximum(running_max, jnp.max(scores, axis=-1))
        weights = jnp.exp(scores - new_max[..., None])
        factor = jnp.exp(running_max - new_max)
        new_sum = running_sum * factor + jnp.sum(weights, axis=-1)
        added = jnp.einsum(
            "gqk,kgd->gqd",
            weights.astype(jnp.bfloat16),
            value_3d,
            preferred_element_type=jnp.float32,
        )
        return (new_max, new_sum, accum * factor[..., None] + added)

    final_max, final_sum, final_acc = lax.fori_loop(0, count // block, one_block, start_state)
    attn_local = (final_acc / final_sum[..., None]).astype(jnp.bfloat16)
    attn_local = attn_local.reshape(kv_local, group, tok_local, width).transpose(2, 0, 1, 3)
    attn_local = attn_local.reshape(tok_local, kv_local * group * width)
    all_heads = lax.all_to_all(attn_local, "tp", split_axis=0, concat_axis=1, tiled=True)
    projected = jnp.dot(all_heads, out_proj, preferred_element_type=jnp.float32)
    hidden1 = (residual.astype(jnp.float32) + projected).astype(jnp.bfloat16)
    hidden_f = hidden1.astype(jnp.float32)
    normed = (
        hidden_f
        * lax.rsqrt(jnp.mean(hidden_f * hidden_f, axis=-1, keepdims=True) + EPS)
        * norm_gain
    ).astype(jnp.bfloat16)
    rows_local = normed.shape[0]
    top_count = routes.shape[1]
    pair_count = rows_local * top_count
    expert_total = expert_gate.shape[0] * lax.axis_size("sp") * lax.axis_size("tp")
    capacity = max(2, 2 * rows_local * top_count // expert_total)
    flat_routes = routes.reshape(pair_count)
    one_hot = (flat_routes[:, None] == jnp.arange(expert_total, dtype=jnp.int32)[None, :]).astype(
        jnp.float32
    )
    lower = (jnp.arange(pair_count)[:, None] >= jnp.arange(pair_count)[None, :]).astype(jnp.float32)
    running_count = jnp.dot(lower, one_hot, precision=lax.Precision.HIGHEST)
    slot_place = (jnp.sum(running_count * one_hot, axis=1) - 1.0).astype(jnp.int32)
    slot_index = flat_routes * capacity + slot_place
    slot_total = expert_total * capacity
    placement = (jnp.arange(slot_total, dtype=jnp.int32)[:, None] == slot_index[None, :]).astype(
        jnp.bfloat16
    )
    placement = jnp.sum(placement.reshape(slot_total, rows_local, top_count), axis=2)
    send_rows = jnp.dot(placement, normed, preferred_element_type=jnp.float32).astype(jnp.bfloat16)
    send_rows = send_rows.reshape(expert_total, capacity, normed.shape[1])
    shared_hidden = (
        jax.nn.silu(jnp.dot(normed, shared_gate, preferred_element_type=jnp.float32))
        * jnp.dot(normed, shared_up, preferred_element_type=jnp.float32)
    ).astype(jnp.bfloat16)
    shared_out = jnp.dot(shared_hidden, shared_down, preferred_element_type=jnp.float32)
    processed = expert_apply(
        lax.all_to_all(send_rows, ("sp", "tp"), split_axis=0, concat_axis=0, tiled=True),
        expert_gate,
        expert_up,
        expert_down,
    )
    returned = lax.all_to_all(processed, ("sp", "tp"), split_axis=0, concat_axis=0, tiled=True)
    returned = returned.reshape(slot_total, normed.shape[1])
    routed = (
        returned[slot_index].reshape(rows_local, top_count, normed.shape[1]).astype(jnp.float32)
    )
    mixed = jnp.einsum("tk,tkd->td", route_weight, routed) + shared_out
    return (hidden_f + mixed).astype(jnp.bfloat16)


def solution(mesh):
    placed = (
        P("sp", "tp"),
        P("sp", "tp"),
        P("sp", "tp"),
        P(("sp", "tp"), None),
        P(),
        P(),
        P(),
        P(),
        P(("sp", "tp"), None),
        P(("sp", "tp"), None),
        P(("sp", "tp"), None, None),
        P(("sp", "tp"), None, None),
        P(("sp", "tp"), None, None),
        P(),
        P(),
        P(),
    )
    return jax.shard_map(
        body, mesh=mesh, in_specs=placed, out_specs=P(("sp", "tp"), None), check_vma=False
    )
```

profile of v0, /device:TPU:0, one launch (start us, length us, event | category | flops | bytes accessed | tf_op | source)
XLA Modules:
  0.0 420.8 jit_solution(3090994777994951920)
XLA Ops:
  19.2 32.9 %all-gather.6.cloned.1.call-done = bf16[4096,1,128]{0,2,1:T(8,128)(2,1)} async-done(((bf16[512,1,128]{0,2,1:T(8,128)(2,1)}), bf16[4096,1,128]{0,2,1:T(8,128)(2,1)}) %all-gather.6.cloned.1.call-update) | async-done | bytes 1048592 | tf_op jit(solution)/shard_map/all_gather | solution.py:92
  52.1 41.4 %all-gather.4.cloned.1.call-done = bf16[4096,128]{1,0:T(8,128)(2,1)} async-done(((bf16[512,128]{1,0:T(8,128)(2,1)}), bf16[4096,128]{1,0:T(8,128)(2,1)}) %all-gather.4.cloned.1.call-update) | async-done | bytes 1048592 | tf_op jit(solution)/shard_map/all_gather | solution.py:93
  93.6 73.7 %while.18 = (s32[]{:T(128)}, f32[1,2048]{1,0:T(1,128)S(1)}, f32[1,2048]{1,0:T(1,128)S(1)}, f32[1,2048,128]{2,1,0:T(8,128)S(1)}, bf16[4096,128]{0,1:T(8,128)(2,1)...) while((s32[]{:T(128)}, f32[1,2048]{1,0:T(1,128)S(1)}, ...), condition=%wide.region_5.6_spmd.clone, body=%wide.region_2.5_spmd.clone.sunk | while | flops 546056192 | bytes 32374984 | solution.py:118
  93.6 3.6 multiply_reduce_fusion.4
  97.2 3.0 fusion.96
  102.8 3.6 multiply_reduce_fusion.4
  106.4 3.0 fusion.96
  112.0 3.6 multiply_reduce_fusion.4
  115.6 3.0 fusion.96
  119.0 2.1 fusion.98
  121.2 3.6 multiply_reduce_fusion.4
  124.8 3.0 fusion.96
  130.4 3.6 multiply_reduce_fusion.4
  134.1 3.0 fusion.96
  139.7 3.6 multiply_reduce_fusion.4
  143.3 3.0 fusion.96
  148.9 3.6 multiply_reduce_fusion.4
  152.5 3.0 fusion.96
  158.1 3.6 multiply_reduce_fusion.4
  161.7 3.0 fusion.96
  169.1 3.7 all-to-all-start
  173.2 8.1 %all-to-all-done = bf16[4,128,512]{2,1,0:T(8,128)(2,1)S(1)} async-done(((bf16[4,128,512]{2,1,0:T(8,128)(2,1)}), bf16[4,128,512]{2,1,0:T(8,128)(2,1)S(1)}, u32[]{:S(2)}, u32[]{:S(2)}) %all-to-all-start) | async-done | bytes 524320 | tf_op jit(solution)/shard_map/all_to_all | solution.py:122
  181.6 4.7 %multiply_reduce_fusion.1 = (f32[128]{0:T(128)S(1)}, f32[128,2048]{1,0:T(8,128)S(1)}) fusion(bf16[128,2048]{0,1:T(8,128)(2,1)S(1)} %bitcast.106, bf16[2048,2048]{1,0:T(8,128)(2,1)} %param.22, bf16[128,2048]{1,0:T(8,128)(2,1)S(1)} %copy-done.5), kind=kOutput, calls=%fused_computation.52 | convolution fusion | flops 1075314560 | bytes 10486272 | tf_op jit(solution)/shard_map/dot_general | solution.py:123
  187.8 95.8 %all_to_all.29 = bf16[32,32,2048]{2,1,0:T(8,128)(2,1)S(1)} all-to-all(bf16[32,32,2048]{2,1,0:T(8,128)(2,1)S(1)} %bitcast.103), channel_id=1, replica_groups=mesh['sp'=8,'tp'=4] {'sp','tp'}, dimensions={0} | all-to-all | bytes 8388608 | tf_op jit(solution)/shard_map/all_to_all | solution.py:157
  285.6 2.3 convolution_bitcast_fusion.2
  287.9 9.1 %convolution_convert_fusion = bf16[32,32,2048]{2,1,0:T(8,128)(2,1)} fusion(bf16[32,32,2048]{2,1,0:T(8,128)(2,1)} %copy-done.2, bf16[1,256,2048]{2,1,0:T(8,128)(2,1)S(1)} %copy-done, bf16[1,2048,256]{2,1,0:T(8,128)(2,1)} %param.29, f32[32,1,32,256]{3,2,0,1:T(8,128)} %convolution_bitcast_fusion.2), kind=kOutput, calls=%fused_computation.23 | convolution fusion | flops 2151153664 | bytes 11534336 | tf_op jit(solution)/shard_map/secf,efh->sech/dot_general | solution.py:55
  297.0 4.0 all-to-all-start.2
  301.7 93.0 %all-to-all-done.2 = bf16[32,32,2048]{2,1,0:T(8,128)(2,1)} async-done(((bf16[32,32,2048]{2,1,0:T(8,128)(2,1)}), bf16[32,32,2048]{2,1,0:T(8,128)(2,1)}, u32[]{:S(2)}, u32[]{:S(2)}) %all-to-all-start.2) | async-done | bytes 4194336 | tf_op jit(solution)/shard_map/all_to_all | solution.py:162
  394.7 8.0 %gather_fusion = bf16[512,2048]{1,0:T(8,128)(2,1)} fusion(bf16[1024,2048]{1,0:T(8,128)(2,1)} %bitcast.29, s32[1024]{0:T(1024)S(1)} %pad_clamp_fusion), kind=kCustom, calls=%fused_computation | custom fusion | bytes 4196352 | tf_op jit(solution)/shard_map/gather | solution.py:165
  402.7 4.2 reshape.478
  406.9 3.8 fusion.76
  410.7 3.3 fusion.19
  (109 shorter events, 37.1 us)
Async XLA Ops:
  6.5 281.3 %copy-start = (bf16[1,256,2048]{2,1,0:T(8,128)(2,1)S(1)}, bf16[1,256,2048]{2,1,0:T(8,128)(2,1)}, u32[]{:S(2)}) copy-start(bf16[1,256,2048]{2,1,0:T(8,128)(2,1)} %param.30) | copy-start | bytes 3145732
  6.5 7.9 %copy-start.9 = (f32[128]{0:T(128)S(1)}, f32[128]{0:T(128)}, u32[]{:S(2)}) copy-start(f32[128]{0:T(128)} %param.23) | copy-start | bytes 1540
  6.5 45.6 %all-gather.6.cloned.1.call-start = ((), (), s32[]{:S(2)}) async-start(), calls=%async_computation.4 | async-start | bytes 1179648 | tf_op jit(solution)/shard_map/all_gather | solution.py:92
  9.7 83.8 %all-gather.4.cloned.1.call-start = ((), (), s32[]{:S(2)}) async-start(), calls=%async_computation.3 | async-start | bytes 1179648 | tf_op jit(solution)/shard_map/all_gather | solution.py:93
  15.2 3.5 copy-start.7
  97.2 3.4 copy-start.1
  106.4 3.4 copy-start.1
  115.6 3.4 copy-start.1
  124.8 3.4 copy-start.1
  134.0 3.4 copy-start.1
  143.3 3.4 copy-start.1
  152.5 3.4 copy-start.1
  161.7 3.4 copy-start.1
  167.3 14.3 %copy-start.5 = (bf16[128,2048]{1,0:T(8,128)(2,1)S(1)}, bf16[128,2048]{1,0:T(8,128)(2,1)}, u32[]{:S(2)}) copy-start(bf16[128,2048]{1,0:T(8,128)(2,1)} %param.21) | copy-start | bytes 1572868
  169.1 12.3 %all-to-all-start = ((bf16[4,128,512]{2,1,0:T(8,128)(2,1)}), bf16[4,128,512]{2,1,0:T(8,128)(2,1)S(1)}, u32[]{:S(2)}, u32[]{:S(2)}) async-start(bf16[4,128,512]{2,1,0:T(8,128)(2,1)} %all_to_all.20), calls=%async_computation | async-start | bytes 1048576 | tf_op jit(solution)/shard_map/all_to_all | solution.py:122
  181.6 4.8 %copy-start.6 = (f32[2048]{0:T(1024)S(1)}, f32[2048]{0:T(1024)}, u32[]{:S(2)}) copy-start(f32[2048]{0:T(1024)} %param.25) | copy-start | bytes 24580
  187.7 97.8 %copy-start.10 = (bf16[1,2048,256]{2,1,0:T(8,128)(2,1)S(1)}, bf16[1,2048,256]{2,1,0:T(8,128)(2,1)}, u32[]{:S(2)}) copy-start(bf16[1,2048,256]{2,1,0:T(8,128)(2,1)} %param.28) | copy-start | bytes 3145732
  283.6 2.0 copy-start.2
  297.0 4.1 copy-start.8
  297.0 4.3 %copy-start.4 = (bf16[2048,256]{1,0:T(8,128)(2,1)S(1)}, bf16[2048,256]{1,0:T(8,128)(2,1)}, u32[]{:S(2)}) copy-start(bf16[2048,256]{1,0:T(8,128)(2,1)} %param.31) | copy-start | bytes 3145732
  297.0 97.7 %all-to-all-start.2 = ((bf16[32,32,2048]{2,1,0:T(8,128)(2,1)}), bf16[32,32,2048]{2,1,0:T(8,128)(2,1)}, u32[]{:S(2)}, u32[]{:S(2)}) async-start(bf16[32,32,2048]{2,1,0:T(8,128)(2,1)} %convolution_convert_fusion), calls=%async_computation.2 | async-start | bytes 8388608 | tf_op jit(solution)/shard_map/all_to_all | solution.py:162
  402.7 8.0 %copy-start.3 = (bf16[256,2048]{1,0:T(8,128)(2,1)S(1)}, bf16[256,2048]{1,0:T(8,128)(2,1)}, u32[]{:S(2)}) copy-start(bf16[256,2048]{1,0:T(8,128)(2,1)} %param.33) | copy-start | bytes 3145732
Sparse Core Ops, SparseCore 0:
  9.9 42.2 all-gather.5
  54.2 39.2 all-gather.3
where the time goes:
time: 422 us; the launch traced here: 421 us
  waiting for transfers between devices  176 us (42%)
  blocking collectives  95.8 us (23%)
  matrix products  71 us (17%)
  other arithmetic  34.1 us (8%)
  local copies, waits for them, and re-layouts  21.8 us (5%)
  between operations  13.7 us (3%)
  starting transfers between devices  7.71 us (2%)
    all_to_all x1, blocking collectives, body(): lax.all_to_all(send_rows, ('sp', 'tp'), split_axis=0, concat_axis=0, tile...  95.8 us
    all_to_all x1, waiting for transfers between devices, body(): lax.all_to_all(processed, ('sp', 'tp'), split_axis=0, concat_axis=0, tile...  93 us
    all_gather x1, waiting for transfers between devices, body(): value_piece = lax.all_gather(values, 'sp', axis=0, tiled=True)  41.4 us
    all_gather x1, waiting for transfers between devices, body(): key_piece = lax.all_gather(k_rot, 'sp', axis=0, tiled=True)  32.9 us
    dot_general x8, matrix products, one_block(): jnp.einsum('gqd,kgd->gqk', query_3d, key_3d, preferred_element_type=jnp.f...  28.8 us
    reduce_sum x8, other arithmetic, one_block(): new_sum = running_sum * factor + jnp.sum(weights, axis=-1)  24.4 us
    dot_general x8, matrix products, one_block(): jnp.einsum('gqk,kgd->gqd', weights.astype(jnp.bfloat16), value_3d, prefer...  17.1 us
    dot_general x1, matrix products, expert_apply(): jnp.einsum('secf,efh->sech', hidden_e, expert_down, preferred_element_typ...  9.08 us
  transfers between devices with their start and end apart: 4, of which 4 were waited for; matrix products, arithmetic and copies ran while one was open for 2% of the time, Pallas kernels for 0%

commit v1 on v0

--- a/solution.py
+++ b/solution.py
@@ -90,7 +90,13 @@
         jnp.zeros((kv_local, group * tok_local, width), jnp.float32),
     )
     key_piece = lax.all_gather(k_rot, "sp", axis=0, tiled=True)
-    value_piece = lax.all_gather(values, "sp", axis=0, tiled=True)
+    size = lax.axis_size("sp")
+    held, tiles = (values, [values])
+    for _ in range(size - 1):
+        held = lax.ppermute(held, "sp", [(i, (i + 1) % size) for i in range(size)])
+        tiles.insert(0, held)
+    line = jnp.concatenate(tiles, axis=0)
+    value_piece = jnp.roll(line, (lax.axis_index("sp") + 1) * values.shape[0], axis=0)
     count = key_piece.shape[0]
     block = math.gcd(count, 512)
 

time: 422 us -> 403 us (0.955)
  waiting for transfers between devices: 176 us -> 145 us
  local copies, waits for them, and re-layouts: 21.8 us -> 31 us
    ppermute x0 -> x7, waiting for transfers between devices: none -> 43.7 us  [body(): held = lax.ppermute(held, 'sp', [(i, (i + 1) % size) for i in range(size)])]
    all_gather x1 -> x0, waiting for transfers between devices: 41.4 us -> none  [body(): value_piece = lax.all_gather(values, 'sp', axis=0, tiled=True)]
    all_gather x1, waiting for transfers between devices: 32.9 us -> 0.01 us  [body(): key_piece = lax.all_gather(k_rot, 'sp', axis=0, tiled=True)]
    unnamed x23 -> x50, local copies, waits for them, and re-layouts: 3.38 us -> 11.6 us
  transfers between devices with their start and end apart: 4 -> 10, of which waited for: 4 -> 9; matrix products, arithmetic and copies ran while one was open for 2% -> 6% of each run, Pallas kernels for 0% -> 0%
where the time goes in v1:
time: 403 us; the launch traced here: 402 us
  waiting for transfers between devices  145 us (36%)
  blocking collectives  95.5 us (24%)
  matrix products  71.7 us (18%)
  other arithmetic  34.1 us (8%)
  local copies, waits for them, and re-layouts  31 us (8%)
  between operations  13.9 us (3%)
  starting transfers between devices  10.2 us (3%)
    all_to_all x1, blocking collectives, body(): lax.all_to_all(send_rows, ('sp', 'tp'), split_axis=0, concat_axis=0, tile...  95.5 us
    all_to_all x1, waiting for transfers between devices, body(): lax.all_to_all(processed, ('sp', 'tp'), split_axis=0, concat_axis=0, tile...  93 us
    ppermute x7, waiting for transfers between devices, body(): held = lax.ppermute(held, 'sp', [(i, (i + 1) % size) for i in range(size)])  43.7 us
    dot_general x8, matrix products, one_block(): jnp.einsum('gqd,kgd->gqk', query_3d, key_3d, preferred_element_type=jnp.f...  28.8 us
    reduce_sum x8, other arithmetic, one_block(): new_sum = running_sum * factor + jnp.sum(weights, axis=-1)  24.4 us
    dot_general x8, matrix products, one_block(): jnp.einsum('gqk,kgd->gqd', weights.astype(jnp.bfloat16), value_3d, prefer...  17.1 us
    unnamed x50, local copies, waits for them, and re-layouts  11.6 us
    dot_general x1, matrix products, expert_apply(): jnp.einsum('secf,efh->sech', hidden_e, expert_down, preferred_element_typ...  9.08 us
  transfers between devices with their start and end apart: 10, of which 9 were waited for; matrix products, arithmetic and copies ran while one was open for 6% of the time, Pallas kernels for 0%

profile of v1, /device:TPU:0, one launch (start us, length us, event | category | flops | bytes accessed | tf_op | source)
XLA Modules:
  0.0 401.8 jit_solution(1445348401114704467)
XLA Ops:
  16.9 7.1 %collective-permute-done.1 = bf16[512,128]{1,0:T(8,128)(2,1)S(1)} collective-permute-done((bf16[512,128]{1,0:T(8,128)(2,1)S(1)}, bf16[512,128]{1,0:T(8,128)(2,1)S(1)}, u32[]{:S(2)}, u32[]{:S(2)}) %collective-permute-start.1) | collective-permute-done | bytes 131104 | tf_op jit(solution)/shard_map/ppermute | solution.py:96
  24.0 9.0 %collective-permute-done.2 = bf16[512,128]{1,0:T(8,128)(2,1)S(1)} collective-permute-done((bf16[512,128]{1,0:T(8,128)(2,1)S(1)}, bf16[512,128]{1,0:T(8,128)(2,1)S(1)}, u32[]{:S(2)}, u32[]{:S(2)}) %collective-permute-start.2) | collective-permute-done | bytes 131104 | tf_op jit(solution)/shard_map/ppermute | solution.py:96
  33.8 6.9 %collective-permute-done.3 = bf16[512,128]{1,0:T(8,128)(2,1)S(1)} collective-permute-done((bf16[512,128]{1,0:T(8,128)(2,1)S(1)}, bf16[512,128]{1,0:T(8,128)(2,1)S(1)}, u32[]{:S(2)}, u32[]{:S(2)}) %collective-permute-start.3) | collective-permute-done | bytes 131104 | tf_op jit(solution)/shard_map/ppermute | solution.py:96
  42.6 7.8 %collective-permute-done.4 = bf16[512,128]{1,0:T(8,128)(2,1)S(1)} collective-permute-done((bf16[512,128]{1,0:T(8,128)(2,1)S(1)}, bf16[512,128]{1,0:T(8,128)(2,1)S(1)}, u32[]{:S(2)}, u32[]{:S(2)}) %collective-permute-start.4) | collective-permute-done | bytes 131104 | tf_op jit(solution)/shard_map/ppermute | solution.py:96
  52.2 6.2 %collective-permute-done.5 = bf16[512,128]{1,0:T(8,128)(2,1)} collective-permute-done((bf16[512,128]{1,0:T(8,128)(2,1)S(1)}, bf16[512,128]{1,0:T(8,128)(2,1)}, u32[]{:S(2)}, u32[]{:S(2)}) %collective-permute-start.5) | collective-permute-done | bytes 131104 | tf_op jit(solution)/shard_map/ppermute | solution.py:96
  62.0 4.4 %collective-permute-done.6 = bf16[512,128]{1,0:T(8,128)(2,1)} collective-permute-done((bf16[512,128]{1,0:T(8,128)(2,1)}, bf16[512,128]{1,0:T(8,128)(2,1)}, u32[]{:S(2)}, u32[]{:S(2)}) %collective-permute-start.6) | collective-permute-done | bytes 131104 | tf_op jit(solution)/shard_map/ppermute | solution.py:96
  75.1 73.8 %while.18 = (s32[]{:T(128)}, f32[1,2048]{1,0:T(1,128)S(1)}, f32[1,2048]{1,0:T(1,128)S(1)}, f32[1,2048,128]{2,1,0:T(8,128)S(1)}, bf16[4096,128]{0,1:T(8,128)(2,1)...) while((s32[]{:T(128)}, f32[1,2048]{1,0:T(1,128)S(1)}, ...), condition=%wide.region_5.6_spmd.clone, body=%wide.region_2.5_spmd.clone.sunk | while | flops 546056192 | bytes 32374992 | solution.py:124
  75.1 3.6 multiply_reduce_fusion.4
  78.7 3.0 fusion.96
  84.3 3.6 multiply_reduce_fusion.4
  88.0 3.0 fusion.96
  93.6 3.6 multiply_reduce_fusion.4
  97.2 3.0 fusion.96
  102.8 3.6 multiply_reduce_fusion.4
  106.4 3.0 fusion.96
  112.0 3.6 multiply_reduce_fusion.4
  121.3 3.6 multiply_reduce_fusion.4
  124.9 3.0 fusion.96
  130.5 3.6 multiply_reduce_fusion.4
  134.1 3.0 fusion.96
  139.7 3.6 multiply_reduce_fusion.4
  150.7 3.5 all-to-all-start
  154.7 8.3 %all-to-all-done = bf16[4,128,512]{2,1,0:T(8,128)(2,1)S(1)} async-done(((bf16[4,128,512]{2,1,0:T(8,128)(2,1)}), bf16[4,128,512]{2,1,0:T(8,128)(2,1)S(1)}, u32[]{:S(2)}, u32[]{:S(2)}) %all-to-all-start) | async-done | bytes 524320 | tf_op jit(solution)/shard_map/all_to_all | solution.py:128
  163.3 4.7 %multiply_reduce_fusion.1 = (f32[128]{0:T(128)S(1)}, f32[128,2048]{1,0:T(8,128)S(1)}) fusion(bf16[128,2048]{0,1:T(8,128)(2,1)S(1)} %bitcast.106, bf16[2048,2048]{1,0:T(8,128)(2,1)} %param.22, bf16[128,2048]{1,0:T(8,128)(2,1)S(1)} %copy-done.5), kind=kOutput, calls=%fused_computation.52 | convolution fusion | flops 1075314560 | bytes 10486272 | tf_op jit(solution)/shard_map/dot_general | solution.py:129
  169.4 95.5 %all_to_all.29 = bf16[32,32,2048]{2,1,0:T(8,128)(2,1)S(1)} all-to-all(bf16[32,32,2048]{2,1,0:T(8,128)(2,1)S(1)} %bitcast.103), channel_id=1, replica_groups=mesh['sp'=8,'tp'=4] {'sp','tp'}, dimensions={0} | all-to-all | bytes 8388608 | tf_op jit(solution)/shard_map/all_to_all | solution.py:163
  269.2 9.1 %convolution_convert_fusion = bf16[32,32,2048]{2,1,0:T(8,128)(2,1)} fusion(bf16[32,32,2048]{2,1,0:T(8,128)(2,1)} %copy-done.2, bf16[1,256,2048]{2,1,0:T(8,128)(2,1)S(1)} %copy-done, bf16[1,2048,256]{2,1,0:T(8,128)(2,1)} %param.29, f32[32,1,32,256]{3,2,0,1:T(8,128)} %convolution_bitcast_fusion.2), kind=kOutput, calls=%fused_computation.23 | convolution fusion | flops 2151153664 | bytes 11534336 | tf_op jit(solution)/shard_map/secf,efh->sech/dot_general | solution.py:55
  278.3 3.7 all-to-all-start.2
  282.7 93.0 %all-to-all-done.2 = bf16[32,32,2048]{2,1,0:T(8,128)(2,1)} async-done(((bf16[32,32,2048]{2,1,0:T(8,128)(2,1)}), bf16[32,32,2048]{2,1,0:T(8,128)(2,1)}, u32[]{:S(2)}, u32[]{:S(2)}) %all-to-all-start.2) | async-done | bytes 4194336 | tf_op jit(solution)/shard_map/all_to_all | solution.py:168
  375.7 8.0 %gather_fusion = bf16[512,2048]{1,0:T(8,128)(2,1)} fusion(bf16[1024,2048]{1,0:T(8,128)(2,1)} %bitcast.29, s32[1024]{0:T(1024)S(1)} %pad_clamp_fusion), kind=kCustom, calls=%fused_computation | custom fusion | bytes 4196352 | tf_op jit(solution)/shard_map/gather | solution.py:171
  383.7 4.1 %reshape.478 = bf16[128,4,2048]{2,1,0:T(4,128)(2,1)} reshape(bf16[512,2048]{1,0:T(8,128)(2,1)} %gather_fusion) | data formatting | bytes 4194304 | tf_op jit(solution)/shard_map/reshape | solution.py:171
  387.8 3.9 fusion.76
  391.7 3.3 fusion.19
  (149 shorter events, 62.0 us)
Async XLA Ops:
  6.5 262.7 %copy-start = (bf16[1,256,2048]{2,1,0:T(8,128)(2,1)S(1)}, bf16[1,256,2048]{2,1,0:T(8,128)(2,1)}, u32[]{:S(2)}) copy-start(bf16[1,256,2048]{2,1,0:T(8,128)(2,1)} %param.30) | copy-start | bytes 3145732
  6.5 68.6 %all-gather.3.cloned.1.call-start = ((), (), s32[]{:S(2)}) async-start(), calls=%async_computation.3 | async-start | bytes 1179648 | tf_op jit(solution)/shard_map/all_gather | solution.py:92
  6.5 9.7 %collective-permute-start = (bf16[512,128]{1,0:T(8,128)(2,1)}, bf16[512,128]{1,0:T(8,128)(2,1)S(1)}, u32[]{:S(2)}, u32[]{:S(2)}) collective-permute-start(bf16[512,128]{1,0:T(8,128)(2,1)} %param.20), channel_id=1, source_target_pairs={{0,4},{4,8},{8,12},{12,16},{16,20},{20,24},{24,28},{28,0},{1,5},{5... | collective-permute-start | bytes 393224 | tf_op jit(solution)/shard_map/ppermute | solution.py:96
  11.4 21.6 %copy-start.15 = (f32[128]{0:T(128)S(1)}, f32[128]{0:T(128)}, u32[]{:S(2)}) copy-start(f32[128]{0:T(128)} %param.23) | copy-start | bytes 1540
  16.3 7.7 %collective-permute-start.1 = (bf16[512,128]{1,0:T(8,128)(2,1)S(1)}, bf16[512,128]{1,0:T(8,128)(2,1)S(1)}, u32[]{:S(2)}, u32[]{:S(2)}) collective-permute-start(bf16[512,128]{1,0:T(8,128)(2,1)S(1)} %collective-permute-done), channel_id=1, source_target_pairs={{0,4},{4,8},{8,12},{12,16},{16,20},{20,24},{24,28},{28,0},{1,5},{5... | collective-permute-start | bytes 393224 | tf_op jit(solution)/shard_map/ppermute | solution.py:96
  24.0 9.1 %collective-permute-start.2 = (bf16[512,128]{1,0:T(8,128)(2,1)S(1)}, bf16[512,128]{1,0:T(8,128)(2,1)S(1)}, u32[]{:S(2)}, u32[]{:S(2)}) collective-permute-start(bf16[512,128]{1,0:T(8,128)(2,1)S(1)} %collective-permute-done.1), channel_id=1, source_target_pairs={{0,4},{4,8},{8,12},{12,16},{16,20},{20,24},{24,28},{28,0},{1,5},{5... | collective-permute-start | bytes 393224 | tf_op jit(solution)/shard_map/ppermute | solution.py:96
  33.0 19.2 %copy-start.7 = (bf16[512,128]{1,0:T(8,128)(2,1)}, bf16[512,128]{1,0:T(8,128)(2,1)S(1)}, u32[]{:S(2)}) copy-start(bf16[512,128]{1,0:T(8,128)(2,1)S(1)} %collective-permute-done.2) | copy-start | bytes 393220
  33.0 7.7 %collective-permute-start.3 = (bf16[512,128]{1,0:T(8,128)(2,1)S(1)}, bf16[512,128]{1,0:T(8,128)(2,1)S(1)}, u32[]{:S(2)}, u32[]{:S(2)}) collective-permute-start(bf16[512,128]{1,0:T(8,128)(2,1)S(1)} %collective-permute-done.2), channel_id=1, source_target_pairs={{0,4},{4,8},{8,12},{12,16},{16,20},{20,24},{24,28},{28,0},{1,5},{5... | collective-permute-start | bytes 393224 | tf_op jit(solution)/shard_map/ppermute | solution.py:96
  40.7 11.5 %copy-start.9 = (bf16[512,128]{1,0:T(8,128)(2,1)}, bf16[512,128]{1,0:T(8,128)(2,1)S(1)}, u32[]{:S(2)}) copy-start(bf16[512,128]{1,0:T(8,128)(2,1)S(1)} %collective-permute-done.3) | copy-start | bytes 393220
  40.7 9.7 %collective-permute-start.4 = (bf16[512,128]{1,0:T(8,128)(2,1)S(1)}, bf16[512,128]{1,0:T(8,128)(2,1)S(1)}, u32[]{:S(2)}, u32[]{:S(2)}) collective-permute-start(bf16[512,128]{1,0:T(8,128)(2,1)S(1)} %collective-permute-done.3), channel_id=1, source_target_pairs={{0,4},{4,8},{8,12},{12,16},{16,20},{20,24},{24,28},{28,0},{1,5},{5... | collective-permute-start | bytes 393224 | tf_op jit(solution)/shard_map/ppermute | solution.py:96
  50.4 8.0 %collective-permute-start.5 = (bf16[512,128]{1,0:T(8,128)(2,1)S(1)}, bf16[512,128]{1,0:T(8,128)(2,1)}, u32[]{:S(2)}, u32[]{:S(2)}) collective-permute-start(bf16[512,128]{1,0:T(8,128)(2,1)S(1)} %collective-permute-done.4), channel_id=1, source_target_pairs={{0,4},{4,8},{8,12},{12,16},{16,20},{20,24},{24,28},{28,0},{1,5},{5... | collective-permute-start | bytes 393224 | tf_op jit(solution)/shard_map/ppermute | solution.py:96
  58.4 8.0 %collective-permute-start.6 = (bf16[512,128]{1,0:T(8,128)(2,1)}, bf16[512,128]{1,0:T(8,128)(2,1)}, u32[]{:S(2)}, u32[]{:S(2)}) collective-permute-start(bf16[512,128]{1,0:T(8,128)(2,1)} %collective-permute-done.5), channel_id=1, source_target_pairs={{0,4},{4,8},{8,12},{12,16},{16,20},{20,24},{24,28},{28,0},{1,5},{5... | collective-permute-start | bytes 393224 | tf_op jit(solution)/shard_map/ppermute | solution.py:96
  60.0 11.1 %copy-start.6 = (bf16[512,128]{1,0:T(8,128)(2,1)S(1)}, bf16[512,128]{1,0:T(8,128)(2,1)}, u32[]{:S(2)}) copy-start(bf16[512,128]{1,0:T(8,128)(2,1)} %param.20) | copy-start | bytes 393220
  60.1 13.7 %copy-start.10 = (bf16[512,128]{1,0:T(8,128)(2,1)S(1)}, bf16[512,128]{1,0:T(8,128)(2,1)}, u32[]{:S(2)}) copy-start(bf16[512,128]{1,0:T(8,128)(2,1)} %copy-done.9) | copy-start | bytes 393220
  60.2 13.8 %copy-start.8 = (bf16[512,128]{1,0:T(8,128)(2,1)S(1)}, bf16[512,128]{1,0:T(8,128)(2,1)}, u32[]{:S(2)}) copy-start(bf16[512,128]{1,0:T(8,128)(2,1)} %copy-done.7) | copy-start | bytes 393220
  78.7 3.5 copy-start.1
  88.0 3.5 copy-start.1
  97.2 3.5 copy-start.1
  106.4 3.5 copy-start.1
  115.6 3.5 copy-start.1
  124.9 3.5 copy-start.1
  134.1 3.5 copy-start.1
  143.3 3.5 copy-start.1
  148.9 5.3 %copy-start.14 = (f32[512]{0:T(512)S(1)}, f32[512]{0:T(512)}, u32[]{:S(2)}) copy-start(f32[512]{0:T(512)} %fusion.25) | copy-start | bytes 6148
  149.7 13.5 %copy-start.5 = (bf16[128,2048]{1,0:T(8,128)(2,1)S(1)}, bf16[128,2048]{1,0:T(8,128)(2,1)}, u32[]{:S(2)}) copy-start(bf16[128,2048]{1,0:T(8,128)(2,1)} %param.21) | copy-start | bytes 1572868
  150.7 12.3 %all-to-all-start = ((bf16[4,128,512]{2,1,0:T(8,128)(2,1)}), bf16[4,128,512]{2,1,0:T(8,128)(2,1)S(1)}, u32[]{:S(2)}, u32[]{:S(2)}) async-start(bf16[4,128,512]{2,1,0:T(8,128)(2,1)} %all_to_all.20), calls=%async_computation | async-start | bytes 1048576 | tf_op jit(solution)/shard_map/all_to_all | solution.py:128
  163.3 4.8 %copy-start.12 = (f32[2048]{0:T(1024)S(1)}, f32[2048]{0:T(1024)}, u32[]{:S(2)}) copy-start(f32[2048]{0:T(1024)} %param.25) | copy-start | bytes 24580
  169.4 97.5 %copy-start.16 = (bf16[1,2048,256]{2,1,0:T(8,128)(2,1)S(1)}, bf16[1,2048,256]{2,1,0:T(8,128)(2,1)}, u32[]{:S(2)}) copy-start(bf16[1,2048,256]{2,1,0:T(8,128)(2,1)} %param.28) | copy-start | bytes 3145732
  278.3 3.8 copy-start.13
  278.3 4.0 %copy-start.4 = (bf16[2048,256]{1,0:T(8,128)(2,1)S(1)}, bf16[2048,256]{1,0:T(8,128)(2,1)}, u32[]{:S(2)}) copy-start(bf16[2048,256]{1,0:T(8,128)(2,1)} %param.31) | copy-start | bytes 3145732
  278.3 97.4 %all-to-all-start.2 = ((bf16[32,32,2048]{2,1,0:T(8,128)(2,1)}), bf16[32,32,2048]{2,1,0:T(8,128)(2,1)}, u32[]{:S(2)}, u32[]{:S(2)}) async-start(bf16[32,32,2048]{2,1,0:T(8,128)(2,1)} %convolution_convert_fusion), calls=%async_computation.2 | async-start | bytes 8388608 | tf_op jit(solution)/shard_map/all_to_all | solution.py:168
  387.8 3.9 copy-start.3
  (2 other events, 3.8 us)
Sparse Core Ops, SparseCore 0:
  12.8 43.6 all-gather.2
